TPU v7x, 512 devices: a whole 4x4x16 slice. The times are simulated.
512 devices in a mesh: fs: 16 (over y, x), tp: 32 (over z, core).
Axes of the slice: x: 4, y: 4, z: 16, core: 2. Of those that a mesh axis runs over, the one named last changes fastest.
Arguments:
- normed: bfloat16 [2048, 49152], P('tp', 'fs'), may hold values from -6 to 6
- key_cot: bfloat16 [2048, 49152], P('tp', 'fs'), may hold values from -6 to 6
- first_map: bfloat16 [2048, 49152], P('tp', 'fs'), may hold values from -6 to 6
- second_map: bfloat16 [2048, 49152], P('tp', 'fs'), may hold values from -6 to 6
- lambdas: float32 [8], replicated, may hold values from 0.3 to 0.8
- factor: bfloat16 [2048, 256], replicated, may hold values from -0.125 to 0.125
- key_master: float32 [2048, 2048], P('fs', 'tp'), may hold values from -0.125 to 0.125
- value_master: float32 [2048, 2048], P('fs', 'tp'), may hold values from -0.125 to 0.125
- key_first: float32 [256, 2048], P('fs', 'tp'), may hold values from -6 to 6
- key_second: float32 [256, 2048], P('fs', 'tp'), may hold values from 0.5 to 2
- value_first: float32 [256, 2048], P('fs', 'tp'), may hold values from -6 to 6
- value_second: float32 [256, 2048], P('fs', 'tp'), may hold values from 0.5 to 2
Outputs:
- key_master_new: float32 [2048, 2048], P('fs', 'tp')
- value_master_new: float32 [2048, 2048], P('fs', 'tp')
- key_copy: bfloat16 [2048, 2048], P(None, 'tp')
- value_copy: bfloat16 [2048, 2048], P(None, 'tp')
- key_first_new: float32 [256, 2048], P('fs', 'tp')
- key_second_new: float32 [256, 2048], P('fs', 'tp')
- value_first_new: float32 [256, 2048], P('fs', 'tp')
- value_second_new: float32 [256, 2048], P('fs', 'tp')
All inputs are finite; a program needn't handle non-finite values.
Results may differ from a plain program's by a relative error of at most 0.0012.
Values may be sent and summed in bfloat16 or wider, within the bound.
No kernel may reach another device: no remote copies, remote signals or barrier semaphores. Data moves between devices by JAX's collectives and lax.ppermute only.
A program may use at most 64 MiB of HBM per device.

v0:
```python
import math
import jax
import jax.numpy as jnp
from jax import lax
from jax.sharding import Mesh
from jax.sharding import PartitionSpec as P

VALUE_DIM = 256
TP = ("tp_0", "tp_1")
FS = ("fs_0", "fs_1")
FS_TP = ("fs_0", "fs_1", "tp_0", "tp_1")


def cut_along(shard, dim, size):
    lengths = shard.shape
    pieces = shard.reshape(*lengths[:dim], size, lengths[dim] // size, *lengths[dim + 1 :])
    return jnp.moveaxis(pieces, dim, 0)


def summed_on_arrival(shard, axis, dim):
    size = lax.axis_size(axis)
    pieces = lax.all_to_all(cut_along(shard, dim, size), axis, 0, 0, tiled=True)
    return jnp.sum(pieces, axis=0)


def sent_to_all(shard, axis):
    size = lax.axis_size(axis)
    return lax.all_to_all(
        jnp.broadcast_to(shard[None], (size, *shard.shape)), axis, 0, 0, tiled=True
    )


def in_order(pieces, dim):
    lengths = list(pieces.shape[1:])
    lengths[dim] *= pieces.shape[0]
    return jnp.moveaxis(pieces, 0, dim).reshape(lengths)


def collect(shard, axis, dim):
    pieces = sent_to_all(shard, axis)
    return in_order(pieces, dim)


def over_axes(shard, axes):
    for axis in axes:
        shard = lax.psum(shard, axis)
    return shard


def local(
    normed,
    key_cot,
    first_map,
    second_map,
    lambdas,
    factor,
    key_master,
    value_master,
    key_first,
    key_second,
    value_first,
    value_second,
):
    width = first_map.shape[0]
    key_width = key_cot.shape[0]
    heads = lambdas.shape[0]
    tok_local = normed.shape[1]
    rows_here = lax.axis_index(TP) * width + lax.iota(jnp.int32, width)
    owners = rows_here // VALUE_DIM
    picked = (owners[:, None] == lax.iota(jnp.int32, heads)[None, :]).astype(jnp.float32)
    row_lambda = jnp.sum(picked * lambdas[None, :], axis=1)
    value_cot = (
        first_map.astype(jnp.float32) - row_lambda[:, None] * second_map.astype(jnp.float32)
    ).astype(jnp.bfloat16)
    cotangents = jnp.concatenate([key_cot, value_cot], axis=0)
    norm_scale = 1.0 / math.sqrt(tok_local * lax.axis_size(FS))
    fs_rows = key_master.shape[0]
    factor_rows = lax.dynamic_slice_in_dim(factor, lax.axis_index(FS) * fs_rows, fs_rows, 0).astype(
        jnp.float32
    )
    term = lax.dot_general(
        lax.all_gather(normed, TP, axis=0, tiled=True),
        cotangents,
        (((1,), (1,)), ((), ())),
        preferred_element_type=jnp.float32,
    )
    gradient = summed_on_arrival(term, FS, 0) * norm_scale
    partial_value = lax.dot_general(
        factor_rows, gradient, (((0,), (0,)), ((), ())), precision=lax.Precision.HIGHEST
    )
    small = summed_on_arrival(partial_value, FS, 0)
    first = jnp.concatenate([key_first, value_first], axis=1)
    second = jnp.concatenate([key_second, value_second], axis=1)
    first_new = 0.8 * first + 0.2 * small
    second_new = 0.9 * second + 0.1 * small * small
    direction = first_new / (jnp.sqrt(second_new) + 1e-06)
    directions = collect(direction, FS, 0)
    raw = jnp.dot(factor_rows, directions, precision=lax.Precision.HIGHEST)
    key_raw = raw[:, :key_width]
    value_raw = raw[:, key_width:]
    squares = (
        over_axes(jnp.sum(key_raw * key_raw), FS_TP),
        over_axes(jnp.sum(value_raw * value_raw), FS_TP),
    )
    key_cells = fs_rows * lax.axis_size(FS) * key_width * lax.axis_size(TP)
    value_cells = fs_rows * lax.axis_size(FS) * width * lax.axis_size(TP)
    key_update = key_raw / jnp.sqrt(squares[0] / key_cells + 0.01)
    value_update = value_raw / jnp.sqrt(squares[1] / value_cells + 0.01)
    key_new = 0.998 * key_master - 0.02 * key_update
    value_new = 0.998 * value_master - 0.02 * value_update
    halves = jnp.concatenate([key_new, value_new], axis=1).astype(jnp.bfloat16)
    copies = collect(halves, FS, 0)
    return (
        key_new,
        value_new,
        copies[:, :key_width],
        copies[:, key_width:],
        first_new[:, :key_width],
        second_new[:, :key_width],
        first_new[:, key_width:],
        second_new[:, key_width:],
    )


def solution(mesh):
    split = Mesh(mesh.devices.reshape(4, 4, 16, 2), ("fs_0", "fs_1", "tp_0", "tp_1"))
    placed = (
        P(TP, FS),
        P(TP, FS),
        P(TP, FS),
        P(TP, FS),
        P(),
        P(),
        P(FS, TP),
        P(FS, TP),
        P(FS, TP),
        P(FS, TP),
        P(FS, TP),
        P(FS, TP),
    )
    return jax.shard_map(
        local,
        mesh=split,
        in_specs=placed,
        out_specs=(
            P(FS, TP),
            P(FS, TP),
            P(None, TP),
            P(None, TP),
            P(FS, TP),
            P(FS, TP),
            P(FS, TP),
            P(FS, TP),
        ),
        check_vma=False,
    )
```

profile of v0, /device:TPU:1, one launch (start us, length us, event | category | flops | bytes accessed | tf_op | source)
XLA Modules:
  0.0 239.1 jit_solution(16993545285375096101)
XLA Ops:
  7.2 0.0 copy-start
  7.2 0.0 copy-start.3
  7.2 0.0 copy-start.5
  7.2 0.0 copy-start.4
  7.2 0.0 copy-start.6
  7.2 0.0 copy-start.1
  7.2 0.0 copy-start.2
  7.2 0.0 all-gather.2.cloned.1.call-start
  7.3 0.7 all-gather.2.cloned.1.call-update
  8.0 0.7 select_reduce_fusion
  8.7 1.3 subtract_convert_fusion
  10.0 92.9 %all-gather.2.cloned.1.call-done = bf16[2048,3072]{1,0:T(8,128)(2,1)} async-done(((bf16[64,3072]{1,0:T(8,128)(2,1)}), bf16[2048,3072]{1,0:T(8,128)(2,1)}) %all-gather.2.cloned.1.call-update) | async-done | bytes 12582928 | tf_op jit(solution)/shard_map/all_gather | solution.py:82
  103.0 9.0 %convolution_bitcast_fusion = f32[16,16,8,128]{3,2,1,0:T(8,128)S(1)} fusion(bf16[2048,3072]{1,0:T(8,128)(2,1)} %all-gather.2.cloned.1.call-done, bf16[64,3072]{1,0:T(8,128)(2,1)S(1)} %subtract_convert_fusion, bf16[64,3072]{1,0:T(8,128)(2,1)} %param.13), kind=kOutput, calls=%fused_computation | convolution fusion | flops 1612185600 | bytes 14417920 | tf_op jit(solution)/shard_map/dot_general | solution.py:81
  112.0 1.1 copy.35
  113.1 6.5 %all-to-all-start = ((f32[16,128,128]{1,2,0:T(8,128)}), f32[16,128,128]{1,2,0:T(8,128)S(1)}, u32[]{:S(2)}, u32[]{:S(2)}) async-start(f32[16,128,128]{1,2,0:T(8,128)} %bitcast.10), calls=%async_computation | async-start | bytes 2097152 | tf_op jit(solution)/shard_map/all_to_all | solution.py:22
  119.6 16.4 %all-to-all-done = f32[16,128,128]{1,2,0:T(8,128)S(1)} async-done(((f32[16,128,128]{1,2,0:T(8,128)}), f32[16,128,128]{1,2,0:T(8,128)S(1)}, u32[]{:S(2)}, u32[]{:S(2)}) %all-to-all-start) | async-done | bytes 1048608 | tf_op jit(solution)/shard_map/all_to_all | solution.py:22
  136.1 0.1 reduce_sum.46
  136.1 0.0 copy-done
  136.1 0.3 fusion.3
  136.4 11.1 %all_to_all.20 = f32[16,16,128]{2,1,0:T(8,128)S(1)} all-to-all(f32[16,16,128]{2,1,0:T(8,128)S(1)} %bitcast.13), channel_id=1, replica_groups=mesh['fs_0'=4,'fs_1'=4,'tp_0'=16,'tp_1'=2] {'fs_0','fs_1'}, dimensions={0} | all-to-all | bytes 262144 | tf_op jit(solution)/shard_map/all_to_all | solution.py:22
  147.6 0.0 copy-done.3
  147.6 0.0 copy-done.5
  147.6 0.0 copy-done.4
  147.6 0.0 copy-done.6
  147.6 0.1 add_divide_fusion
  147.7 9.9 %all_to_all.21 = f32[16,16,128]{2,1,0:T(8,128)S(1)} all-to-all(f32[16,16,128]{2,1,0:T(8,128)S(1)} %broadcast_in_dim.4), channel_id=1, replica_groups=mesh['fs_0'=4,'fs_1'=4,'tp_0'=16,'tp_1'=2] {'fs_0','fs_1'}, dimensions={0} | all-to-all | bytes 262144 | tf_op jit(solution)/shard_map/all_to_all | solution.py:28
  157.6 0.3 fusion.5
  157.9 0.6 multiply_reduce_fusion
  158.5 7.3 %all-reduce.2 = (f32[]{:T(128)}, f32[]{:T(128)}) all-reduce(f32[]{:T(128)} %get-tuple-element.25, f32[]{:T(128)} %get-tuple-element.24), channel_id=1, replica_groups=mesh['fs_0'=4,'fs_1'=4,'tp_0'=16,'tp_1'=2] {'fs_0'}, use_global_device_ids=true, to_apply=%region_4.5 | all-reduce | flops 2 | bytes 16 | tf_op jit(solution)/shard_map/psum | solution.py:46
  165.8 7.5 %all-reduce.1 = (f32[]{:T(128)}, f32[]{:T(128)}) all-reduce(f32[]{:T(128)} %get-tuple-element.30, f32[]{:T(128)} %get-tuple-element.31), channel_id=1, replica_groups=mesh['fs_0'=4,'fs_1'=4,'tp_0'=16,'tp_1'=2] {'fs_1'}, use_global_device_ids=true, to_apply=%region_5.6 | all-reduce | flops 2 | bytes 16 | tf_op jit(solution)/shard_map/psum | solution.py:46
  173.3 22.4 %all-reduce = (f32[]{:T(128)}, f32[]{:T(128)}) all-reduce(f32[]{:T(128)} %get-tuple-element.28, f32[]{:T(128)} %get-tuple-element.29), channel_id=1, replica_groups=mesh['fs_0'=4,'fs_1'=4,'tp_0'=16,'tp_1'=2] {'tp_0'}, use_global_device_ids=true, to_apply=%region_6.7 | all-reduce | flops 2 | bytes 16 | tf_op jit(solution)/shard_map/psum | solution.py:46
  195.6 16.8 %all-reduce.3 = (f32[]{:T(128)}, f32[]{:T(128)}) all-reduce(f32[]{:T(128)} %get-tuple-element.26, f32[]{:T(128)} %get-tuple-element.27), channel_id=1, replica_groups=mesh['fs_0'=4,'fs_1'=4,'tp_0'=16,'tp_1'=2] {'tp_1'}, use_global_device_ids=true, to_apply=%region_7.8 | all-reduce | flops 2 | bytes 16 | tf_op jit(solution)/shard_map/psum | solution.py:46
  213.8 0.0 copy-done.1
  213.8 0.0 copy-done.2
  213.8 0.6 fusion.16
  214.5 0.9 broadcast_in_dim.5
  215.4 3.6 %all-to-all-start.3 = ((bf16[16,128,128]{1,2,0:T(8,128)(2,1)}), bf16[16,128,128]{1,2,0:T(8,128)(2,1)S(1)}, u32[]{:S(2)}, u32[]{:S(2)}) async-start(bf16[16,128,128]{1,2,0:T(8,128)(2,1)} %broadcast_in_dim.5), calls=%async_computation.3 | async-start | bytes 1048576 | tf_op jit(solution)/shard_map/all_to_all | solution.py:28
  219.0 0.7 fusion.20
  219.6 10.3 %all-to-all-done.3 = bf16[16,128,128]{1,2,0:T(8,128)(2,1)S(1)} async-done(((bf16[16,128,128]{1,2,0:T(8,128)(2,1)}), bf16[16,128,128]{1,2,0:T(8,128)(2,1)S(1)}, u32[]{:S(2)}, u32[]{:S(2)}) %all-to-all-start.3) | async-done | bytes 524320 | tf_op jit(solution)/shard_map/all_to_all | solution.py:28
  229.9 0.3 copy.29
  230.2 0.2 fusion.19
  230.4 0.9 copy.31
  231.3 0.9 copy.30
  (4 shorter events, 0.0 us)
Async XLA Ops:
  7.2 129.0 %copy-start = (bf16[2048,256]{1,0:T(8,128)(2,1)S(1)}, bf16[2048,256]{1,0:T(8,128)(2,1)}, u32[]{:S(2)}) copy-start(bf16[2048,256]{1,0:T(8,128)(2,1)} %param.17) | copy-start | bytes 3145732
  7.2 140.4 %copy-start.3 = (f32[16,64]{1,0:T(8,128)S(1)}, f32[16,64]{1,0:T(8,128)}, u32[]{:S(2)}) copy-start(f32[16,64]{1,0:T(8,128)} %param.23) | copy-start | bytes 12292
  7.2 140.4 %copy-start.5 = (f32[16,64]{1,0:T(8,128)S(1)}, f32[16,64]{1,0:T(8,128)}, u32[]{:S(2)}) copy-start(f32[16,64]{1,0:T(8,128)} %param.22) | copy-start | bytes 12292
  7.2 140.4 %copy-start.4 = (f32[16,64]{1,0:T(8,128)S(1)}, f32[16,64]{1,0:T(8,128)}, u32[]{:S(2)}) copy-start(f32[16,64]{1,0:T(8,128)} %param.21) | copy-start | bytes 12292
  7.2 140.4 %copy-start.6 = (f32[16,64]{1,0:T(8,128)S(1)}, f32[16,64]{1,0:T(8,128)}, u32[]{:S(2)}) copy-start(f32[16,64]{1,0:T(8,128)} %param.20) | copy-start | bytes 12292
  7.2 206.6 %copy-start.1 = (f32[128,64]{0,1:T(8,128)S(1)}, f32[128,64]{0,1:T(8,128)}, u32[]{:S(2)}) copy-start(f32[128,64]{0,1:T(8,128)} %param.19) | copy-start | bytes 98308
  7.2 206.6 %copy-start.2 = (f32[128,64]{0,1:T(8,128)S(1)}, f32[128,64]{0,1:T(8,128)}, u32[]{:S(2)}) copy-start(f32[128,64]{0,1:T(8,128)} %param.18) | copy-start | bytes 98308
  7.2 95.7 %all-gather.2.cloned.1.call-start = ((), (), s32[]{:S(2)}) async-start(), calls=%async_computation.4 | async-start | bytes 12976128 | tf_op jit(solution)/shard_map/all_gather | solution.py:82
  113.1 23.0 %all-to-all-start = ((f32[16,128,128]{1,2,0:T(8,128)}), f32[16,128,128]{1,2,0:T(8,128)S(1)}, u32[]{:S(2)}, u32[]{:S(2)}) async-start(f32[16,128,128]{1,2,0:T(8,128)} %bitcast.10), calls=%async_computation | async-start | bytes 2097152 | tf_op jit(solution)/shard_map/all_to_all | solution.py:22
  215.4 14.5 %all-to-all-start.3 = ((bf16[16,128,128]{1,2,0:T(8,128)(2,1)}), bf16[16,128,128]{1,2,0:T(8,128)(2,1)S(1)}, u32[]{:S(2)}, u32[]{:S(2)}) async-start(bf16[16,128,128]{1,2,0:T(8,128)(2,1)} %broadcast_in_dim.5), calls=%async_computation.3 | async-start | bytes 1048576 | tf_op jit(solution)/shard_map/all_to_all | solution.py:28
Sparse Core Ops, SparseCore 0:
  10.2 92.7 all-gather.1
where the time goes:
time: 240 us; the launch traced here: 239 us
  waiting for transfers between devices  120 us (50%)
  blocking collectives  74.9 us (31%)
  between operations  15.6 us (6%)
  starting transfers between devices  10.1 us (4%)
  matrix products  9.54 us (4%)
  local copies, waits for them, and re-layouts  5 us (2%)
  other arithmetic  3.48 us (1%)
    all_gather x1, waiting for transfers between devices, local(): lax.all_gather(normed, TP, axis=0, tiled=True)  92.9 us
    psum x4, blocking collectives, over_axes(): shard = lax.psum(shard, axis)  53.9 us
    all_to_all x1, waiting for transfers between devices, summed_on_arrival(): pieces = lax.all_to_all(cut_along(shard, dim, size), axis, 0, 0, tiled=True)  16.4 us
    all_to_all x1, blocking collectives, summed_on_arrival(): pieces = lax.all_to_all(cut_along(shard, dim, size), axis, 0, 0, tiled=True)  11.1 us
    all_to_all x1, waiting for transfers between devices, sent_to_all(): lax.all_to_all(jnp.broadcast_to(shard[None], (size, *shard.shape)), axis,...  10.3 us
    all_to_all x1, blocking collectives, sent_to_all(): lax.all_to_all(jnp.broadcast_to(shard[None], (size, *shard.shape)), axis,...  9.93 us
    dot_general x1, matrix products, local(): lax.dot_general(lax.all_gather(normed, TP, axis=0, tiled=True), cotangent...  8.99 us
    all_to_all x1, starting transfers between devices, summed_on_arrival(): pieces = lax.all_to_all(cut_along(shard, dim, size), axis, 0, 0, tiled=True)  6.53 us
  transfers between devices with their start and end apart: 3, of which 3 were waited for; matrix products, arithmetic and copies ran while one was open for 1% of the time, Pallas kernels for 0%

commit v1 on v0

--- a/solution.py
+++ b/solution.py
@@ -79,7 +79,7 @@
         jnp.float32
     )
     term = lax.dot_general(
-        lax.all_gather(normed, TP, axis=0, tiled=True),
+        jnp.concatenate(lax.all_to_all(jnp.stack([normed] * lax.axis_size(TP)), TP, 0, 0), axis=0),
         cotangents,
         (((1,), (1,)), ((), ())),
         preferred_element_type=jnp.float32,

time: 240 us -> 703 us (2.93)
  waiting for transfers between devices: 120 us -> 564 us
  starting transfers between devices: 10.1 us -> 27.3 us
  between operations: 15.6 us -> 2.24 us
  blocking collectives: 74.9 us -> 85.7 us
  local copies, waits for them, and re-layouts: 5 us -> 12.2 us
    all_to_all x0 -> x1, waiting for transfers between devices: none -> 538 us  [local(): lax.all_to_all(jnp.stack([normed] * lax.axis_size(TP)), TP, 0, 0)]
    all_gather x1 -> x0, waiting for transfers between devices: 92.9 us -> none  [local(): lax.all_gather(normed, TP, axis=0, tiled=True)]
    all_to_all x0 -> x1, starting transfers between devices: none -> 16.9 us  [local(): lax.all_to_all(jnp.stack([normed] * lax.axis_size(TP)), TP, 0, 0)]
    psum x4, blocking collectives: 53.9 us -> 64.6 us  [over_axes(): shard = lax.psum(shard, axis)]
    another operation x0 -> x1, local copies, waits for them, and re-layouts: none -> 7.16 us  [local(): jnp.stack([normed] * lax.axis_size(TP))]
  transfers between devices with their start and end apart: 3 -> 3, of which waited for: 3 -> 3; matrix products, arithmetic and copies ran while one was open for 1% -> 0% of each run, Pallas kernels for 0% -> 0%
where the time goes in v1:
time: 703 us
  waiting for transfers between devices  564 us (80%)
  blocking collectives  85.7 us (12%)
  starting transfers between devices  27.3 us (4%)
  local copies, waits for them, and re-layouts  12.2 us (2%)
  matrix products  9.38 us (1%)
    all_to_all x1, waiting for transfers between devices, local(): lax.all_to_all(jnp.stack([normed] * lax.axis_size(TP)), TP, 0, 0)  538 us
    psum x4, blocking collectives, over_axes(): shard = lax.psum(shard, axis)  64.6 us
    all_to_all x1, starting transfers between devices, local(): lax.all_to_all(jnp.stack([normed] * lax.axis_size(TP)), TP, 0, 0)  16.9 us
    all_to_all x1, waiting for transfers between devices, summed_on_arrival(): pieces = lax.all_to_all(cut_along(shard, dim, size), axis, 0, 0, tiled=True)  16.2 us
  transfers between devices with their start and end apart: 3, of which 3 were waited for; matrix products, arithmetic and copies ran while one was open for 0% of the time, Pallas kernels for 0%

profile of v1, /device:TPU:1, one launch (start us, length us, event | category | flops | bytes accessed | tf_op | source)
XLA Modules:
  0.0 702.8 jit_solution(15912685589081085342)
XLA Ops:
  0.6 0.0 copy-start
  0.6 7.2 %stack.2 = bf16[32,64,3072]{2,1,0:T(8,128)(2,1)} broadcast(bf16[64,3072]{1,0:T(8,128)(2,1)} %param.12), dimensions={1,2} | broadcast | bytes 12976128 | tf_op jit(solution)/shard_map/stack | solution.py:82
  7.8 0.0 copy-start.10
  7.8 0.0 copy-start.2
  7.8 0.0 copy-start.3
  7.8 0.0 copy-start.1
  7.8 16.9 %all-to-all-start = ((bf16[32,64,3072]{2,1,0:T(8,128)(2,1)}), bf16[32,64,3072]{2,1,0:T(8,128)(2,1)}, u32[]{:S(2)}, u32[]{:S(2)}) async-start(bf16[32,64,3072]{2,1,0:T(8,128)(2,1)} %stack.2), calls=%async_computation | async-start | bytes 25165824 | tf_op jit(solution)/shard_map/all_to_all | solution.py:82
  24.8 0.0 copy-start.6
  24.8 0.0 copy-start.7
  24.8 0.0 copy-start.8
  24.8 0.0 copy-start.9
  24.8 0.0 copy-start.4
  24.8 0.0 copy-start.5
  24.9 0.0 copy-done.10
  24.9 0.1 select_reduce_fusion
  25.0 0.0 copy-done.2
  25.0 0.0 copy-done.3
  25.0 0.2 subtract_convert_fusion
  25.1 537.9 %all-to-all-done = bf16[32,64,3072]{2,1,0:T(8,128)(2,1)} async-done(((bf16[32,64,3072]{2,1,0:T(8,128)(2,1)}), bf16[32,64,3072]{2,1,0:T(8,128)(2,1)}, u32[]{:S(2)}, u32[]{:S(2)}) %all-to-all-start) | async-done | bytes 12582944 | tf_op jit(solution)/shard_map/all_to_all | solution.py:82
  563.0 0.0 copy-done.1
  563.0 8.8 %convolution_bitcast_fusion = f32[16,16,8,128]{3,2,1,0:T(8,128)S(1)} fusion(bf16[2048,3072]{1,0:T(8,128)(2,1)} %bitcast, bf16[64,3072]{1,0:T(8,128)(2,1)S(1)} %subtract_convert_fusion, bf16[64,3072]{1,0:T(8,128)(2,1)S(1)} %copy-done.1), kind=kOutput, calls=%fused_computation | convolution fusion | flops 1612185600 | bytes 14417920 | tf_op jit(solution)/shard_map/dot_general | solution.py:81
  571.9 1.1 copy.35
  573.0 6.8 all-to-all-start.1
  579.7 16.2 %all-to-all-done.1 = f32[16,128,128]{1,2,0:T(8,128)S(1)} async-done(((f32[16,128,128]{1,2,0:T(8,128)}), f32[16,128,128]{1,2,0:T(8,128)S(1)}, u32[]{:S(2)}, u32[]{:S(2)}) %all-to-all-start.1) | async-done | bytes 1048608 | tf_op jit(solution)/shard_map/all_to_all | solution.py:22
  595.9 0.1 reduce_sum.46
  596.0 0.0 copy-done
  596.0 0.3 fusion.3
  596.3 11.2 %all_to_all.25 = f32[16,16,128]{2,1,0:T(8,128)S(1)} all-to-all(f32[16,16,128]{2,1,0:T(8,128)S(1)} %bitcast.14), channel_id=1, replica_groups=mesh['fs_0'=4,'fs_1'=4,'tp_0'=16,'tp_1'=2] {'fs_0','fs_1'}, dimensions={0} | all-to-all | bytes 262144 | tf_op jit(solution)/shard_map/all_to_all | solution.py:22
  607.5 0.0 copy-done.6
  607.5 0.0 copy-done.7
  607.5 0.0 copy-done.8
  607.5 0.0 copy-done.9
  607.5 0.1 add_divide_fusion
  607.6 9.9 %all_to_all.26 = f32[16,16,128]{2,1,0:T(8,128)S(1)} all-to-all(f32[16,16,128]{2,1,0:T(8,128)S(1)} %broadcast_in_dim.4), channel_id=1, replica_groups=mesh['fs_0'=4,'fs_1'=4,'tp_0'=16,'tp_1'=2] {'fs_0','fs_1'}, dimensions={0} | all-to-all | bytes 262144 | tf_op jit(solution)/shard_map/all_to_all | solution.py:28
  617.6 0.3 fusion.5
  617.9 0.6 multiply_reduce_fusion
  618.5 7.3 %all-reduce.2 = (f32[]{:T(128)}, f32[]{:T(128)}) all-reduce(f32[]{:T(128)} %get-tuple-element.25, f32[]{:T(128)} %get-tuple-element.24), channel_id=1, replica_groups=mesh['fs_0'=4,'fs_1'=4,'tp_0'=16,'tp_1'=2] {'fs_0'}, use_global_device_ids=true, to_apply=%region_4.5 | all-reduce | flops 2 | bytes 16 | tf_op jit(solution)/shard_map/psum | solution.py:46
  625.7 7.5 %all-reduce.1 = (f32[]{:T(128)}, f32[]{:T(128)}) all-reduce(f32[]{:T(128)} %get-tuple-element.30, f32[]{:T(128)} %get-tuple-element.31), channel_id=1, replica_groups=mesh['fs_0'=4,'fs_1'=4,'tp_0'=16,'tp_1'=2] {'fs_1'}, use_global_device_ids=true, to_apply=%region_5.6 | all-reduce | flops 2 | bytes 16 | tf_op jit(solution)/shard_map/psum | solution.py:46
  633.2 32.1 %all-reduce = (f32[]{:T(128)}, f32[]{:T(128)}) all-reduce(f32[]{:T(128)} %get-tuple-element.28, f32[]{:T(128)} %get-tuple-element.29), channel_id=1, replica_groups=mesh['fs_0'=4,'fs_1'=4,'tp_0'=16,'tp_1'=2] {'tp_0'}, use_global_device_ids=true, to_apply=%region_6.7 | all-reduce | flops 2 | bytes 16 | tf_op jit(solution)/shard_map/psum | solution.py:46
  665.3 17.7 %all-reduce.3 = (f32[]{:T(128)}, f32[]{:T(128)}) all-reduce(f32[]{:T(128)} %get-tuple-element.26, f32[]{:T(128)} %get-tuple-element.27), channel_id=1, replica_groups=mesh['fs_0'=4,'fs_1'=4,'tp_0'=16,'tp_1'=2] {'tp_1'}, use_global_device_ids=true, to_apply=%region_7.8 | all-reduce | flops 2 | bytes 16 | tf_op jit(solution)/shard_map/psum | solution.py:46
  684.4 0.0 copy-done.4
  684.4 0.0 copy-done.5
  684.4 0.6 fusion.16
  685.1 0.9 broadcast_in_dim.5
  686.0 3.6 all-to-all-start.4
  689.5 0.7 fusion.20
  690.2 10.3 %all-to-all-done.4 = bf16[16,128,128]{1,2,0:T(8,128)(2,1)S(1)} async-done(((bf16[16,128,128]{1,2,0:T(8,128)(2,1)}), bf16[16,128,128]{1,2,0:T(8,128)(2,1)S(1)}, u32[]{:S(2)}, u32[]{:S(2)}) %all-to-all-start.4) | async-done | bytes 524320 | tf_op jit(solution)/shard_map/all_to_all | solution.py:28
  700.5 0.3 copy.29
  700.8 0.2 fusion.19
  701.0 0.9 copy.30
  701.9 0.9 copy.31
  (4 shorter events, 0.0 us)
Async XLA Ops:
  0.6 595.4 %copy-start = (bf16[2048,256]{1,0:T(8,128)(2,1)S(1)}, bf16[2048,256]{1,0:T(8,128)(2,1)}, u32[]{:S(2)}) copy-start(bf16[2048,256]{1,0:T(8,128)(2,1)} %param.17) | copy-start | bytes 3145732
  7.8 17.0 %copy-start.10 = (f32[8]{0:T(128)S(1)}, f32[8]{0:T(128)}, u32[]{:S(2)}) copy-start(f32[8]{0:T(128)} %param.16) | copy-start | bytes 100
  7.8 17.1 %copy-start.2 = (bf16[64,3072]{1,0:T(8,128)(2,1)S(1)}, bf16[64,3072]{1,0:T(8,128)(2,1)}, u32[]{:S(2)}) copy-start(bf16[64,3072]{1,0:T(8,128)(2,1)} %param.15) | copy-start | bytes 1179652
  7.8 17.1 %copy-start.3 = (bf16[64,3072]{1,0:T(8,128)(2,1)S(1)}, bf16[64,3072]{1,0:T(8,128)(2,1)}, u32[]{:S(2)}) copy-start(bf16[64,3072]{1,0:T(8,128)(2,1)} %param.14) | copy-start | bytes 1179652
  7.8 555.2 %copy-start.1 = (bf16[64,3072]{1,0:T(8,128)(2,1)S(1)}, bf16[64,3072]{1,0:T(8,128)(2,1)}, u32[]{:S(2)}) copy-start(bf16[64,3072]{1,0:T(8,128)(2,1)} %param.13) | copy-start | bytes 1179652
  7.8 555.2 %all-to-all-start = ((bf16[32,64,3072]{2,1,0:T(8,128)(2,1)}), bf16[32,64,3072]{2,1,0:T(8,128)(2,1)}, u32[]{:S(2)}, u32[]{:S(2)}) async-start(bf16[32,64,3072]{2,1,0:T(8,128)(2,1)} %stack.2), calls=%async_computation | async-start | bytes 25165824 | tf_op jit(solution)/shard_map/all_to_all | solution.py:82
  24.8 582.7 %copy-start.6 = (f32[16,64]{1,0:T(8,128)S(1)}, f32[16,64]{1,0:T(8,128)}, u32[]{:S(2)}) copy-start(f32[16,64]{1,0:T(8,128)} %param.23) | copy-start | bytes 12292
  24.8 582.7 %copy-start.7 = (f32[16,64]{1,0:T(8,128)S(1)}, f32[16,64]{1,0:T(8,128)}, u32[]{:S(2)}) copy-start(f32[16,64]{1,0:T(8,128)} %param.21) | copy-start | bytes 12292
  24.8 582.7 %copy-start.8 = (f32[16,64]{1,0:T(8,128)S(1)}, f32[16,64]{1,0:T(8,128)}, u32[]{:S(2)}) copy-start(f32[16,64]{1,0:T(8,128)} %param.22) | copy-start | bytes 12292
  24.8 582.7 %copy-start.9 = (f32[16,64]{1,0:T(8,128)S(1)}, f32[16,64]{1,0:T(8,128)}, u32[]{:S(2)}) copy-start(f32[16,64]{1,0:T(8,128)} %param.20) | copy-start | bytes 12292
  24.8 659.6 %copy-start.4 = (f32[128,64]{0,1:T(8,128)S(1)}, f32[128,64]{0,1:T(8,128)}, u32[]{:S(2)}) copy-start(f32[128,64]{0,1:T(8,128)} %param.19) | copy-start | bytes 98308
  24.8 659.6 %copy-start.5 = (f32[128,64]{0,1:T(8,128)S(1)}, f32[128,64]{0,1:T(8,128)}, u32[]{:S(2)}) copy-start(f32[128,64]{0,1:T(8,128)} %param.18) | copy-start | bytes 98308
  573.0 23.0 %all-to-all-start.1 = ((f32[16,128,128]{1,2,0:T(8,128)}), f32[16,128,128]{1,2,0:T(8,128)S(1)}, u32[]{:S(2)}, u32[]{:S(2)}) async-start(f32[16,128,128]{1,2,0:T(8,128)} %bitcast.11), calls=%async_computation.1 | async-start | bytes 2097152 | tf_op jit(solution)/shard_map/all_to_all | solution.py:22
  686.0 14.5 %all-to-all-start.4 = ((bf16[16,128,128]{1,2,0:T(8,128)(2,1)}), bf16[16,128,128]{1,2,0:T(8,128)(2,1)S(1)}, u32[]{:S(2)}, u32[]{:S(2)}) async-start(bf16[16,128,128]{1,2,0:T(8,128)(2,1)} %broadcast_in_dim.5), calls=%async_computation.4 | async-start | bytes 1048576 | tf_op jit(solution)/shard_map/all_to_all | solution.py:28
